TPU v7x, 32 devices: a whole 2x2x4 slice. The times are simulated.
32 devices in a mesh: kv: 16 (over z, y, x), tp: 2 (over core).
Axes of the slice: x: 2, y: 2, z: 4, core: 2. Of those that a mesh axis runs over, the one named last changes fastest.
Arguments:
- tokens: bfloat16 [256, 2048], P('kv', 'tp'), may hold values from -20 to 20
- norm_gain: float32 [2048], replicated, may hold values from 0.1 to 1.9
- w_query: bfloat16 [2048, 1024], P(None, 'tp'), may hold values from -0.125 to 0.125
- w_key: bfloat16 [2048, 1024], P(None, 'tp'), may hold values from -0.125 to 0.125
- w_value: bfloat16 [2048, 1024], P(None, 'tp'), may hold values from -0.125 to 0.125
- w_outgate: bfloat16 [2048, 1024], P(None, 'tp'), may hold values from -0.125 to 0.125
- w_input_gate: bfloat16 [2048, 8], replicated, may hold values from -0.125 to 0.125
- w_forget_gate: bfloat16 [2048, 8], replicated, may hold values from -0.125 to 0.125
- memory: float32 [256, 8, 128, 128], P('kv', 'tp'), may hold values from -6 to 6
- normalizer: float32 [256, 8, 128], P('kv', 'tp'), may hold values from -6 to 6
- memory_max: float32 [256, 8], P('kv', 'tp'), may hold values from -2 to 300
- w_output: bfloat16 [1024, 2048], P(None, 'tp'), may hold values from -0.1875 to 0.1875
- ffn_gain: float32 [2048], P('tp'), may hold values from 0.1 to 1.9
- w_gate: bfloat16 [2048, 5632], P('tp', 'kv'), may hold values from -0.125 to 0.125
- w_up: bfloat16 [2048, 5632], P('tp', 'kv'), may hold values from -0.125 to 0.125
- w_down: bfloat16 [5632, 2048], P('kv', 'tp'), may hold values from -0.078125 to 0.078125
Outputs:
- result: bfloat16 [256, 2048], P('kv', 'tp')
- new_memory: float32 [256, 8, 128, 128], P('kv', 'tp')
- new_normalizer: float32 [256, 8, 128], P('kv', 'tp')
- new_max: float32 [256, 8], P('kv', 'tp')
All inputs are finite; a program needn't handle non-finite values.
Results may differ from a plain program's by a relative error of at most 0.013.
Values may be sent and summed in bfloat16 or wider, within the bound.
A program may use at most 64 MiB of HBM per device.

v0:
```python
import jax
import jax.numpy as jnp
from jax import lax
from jax.sharding import PartitionSpec as P

D = 2048


def activate(gate_sum, up_sum, square_sum):
    ffn_scale = lax.rsqrt(square_sum / D + 1e-06)[:, None]
    return (jax.nn.silu(ffn_scale * gate_sum) * (ffn_scale * up_sum)).astype(jnp.bfloat16)


def per_device(
    tokens,
    norm_gain,
    w_query,
    w_key,
    w_value,
    w_outgate,
    w_input_gate,
    w_forget_gate,
    memory,
    normalizer,
    memory_max,
    w_output,
    ffn_gain,
    w_gate,
    w_up,
    w_down,
):
    local_rows = tokens.shape[0]
    head_count = memory.shape[1]
    head_dim = memory.shape[2]
    full_rows = lax.all_gather(tokens, "tp", axis=1, tiled=True)
    rows_f = full_rows.astype(jnp.float32)
    row_scale = lax.rsqrt(jnp.mean(rows_f * rows_f, axis=-1, keepdims=True) + 1e-06)
    normed = (rows_f * row_scale * norm_gain).astype(jnp.bfloat16)

    def project(weight):
        return jnp.dot(normed, weight, preferred_element_type=jnp.float32).reshape(
            local_rows, head_count, head_dim
        )

    queries = project(w_query) * head_dim ** (-0.5)
    key_vec = project(w_key)
    values = project(w_value)
    outgate = project(w_outgate)
    first_head = lax.axis_index("tp") * head_count
    igate = lax.dynamic_slice_in_dim(
        jnp.dot(normed, w_input_gate, preferred_element_type=jnp.float32), first_head, head_count, 1
    )
    forget_pre = lax.dynamic_slice_in_dim(
        jnp.dot(normed, w_forget_gate, preferred_element_type=jnp.float32),
        first_head,
        head_count,
        1,
    )
    lforget = jax.nn.log_sigmoid(forget_pre)
    new_max = jnp.maximum(lforget + memory_max, igate)
    keep_weight = jnp.exp(lforget + memory_max - new_max)
    admit_weight = jnp.exp(igate - new_max)
    new_memory = keep_weight[..., None, None] * memory + admit_weight[..., None, None] * (
        key_vec[..., :, None] * values[..., None, :]
    )
    new_normalizer = keep_weight[..., None] * normalizer + admit_weight[..., None] * key_vec
    numerator = jnp.einsum("bhd,bhdv->bhv", queries, new_memory, precision=lax.Precision.HIGHEST)
    denominator = jnp.sum(queries * new_normalizer, axis=-1)
    cell_out = numerator / jnp.maximum(jnp.abs(denominator), jnp.exp(-new_max))[..., None]
    head_mean = jnp.mean(cell_out, axis=-1, keepdims=True)
    centered = cell_out - head_mean
    head_var = jnp.mean(centered * centered, axis=-1, keepdims=True)
    mixed = (
        (jax.nn.sigmoid(outgate) * centered * lax.rsqrt(head_var + 1e-05))
        .reshape(local_rows, head_count * head_dim)
        .astype(jnp.bfloat16)
    )
    branch_out = jnp.dot(
        lax.all_gather(mixed, "tp", axis=1, tiled=True),
        w_output,
        preferred_element_type=jnp.float32,
    )
    resid = (tokens.astype(jnp.float32) + branch_out).astype(jnp.bfloat16)
    every_row = lax.all_gather(resid, "kv", axis=0, tiled=True)
    every_f = every_row.astype(jnp.float32)
    square_part = jnp.sum(every_f * every_f, axis=-1)
    ffn_in = (every_f * ffn_gain).astype(jnp.bfloat16)
    gate_part = jnp.dot(ffn_in, w_gate, preferred_element_type=jnp.float32)
    up_part = jnp.dot(ffn_in, w_up, preferred_element_type=jnp.float32)
    gate_full, up_full, square_full = (
        lax.psum(gate_part.astype(jnp.bfloat16), "tp").astype(jnp.float32),
        lax.psum(up_part.astype(jnp.bfloat16), "tp").astype(jnp.float32),
        lax.psum(square_part.astype(jnp.bfloat16), "tp").astype(jnp.float32),
    )
    hidden = activate(gate_full, up_full, square_full)
    down_out = lax.psum_scatter(
        jnp.dot(hidden, w_down, preferred_element_type=jnp.float32),
        "kv",
        scatter_dimension=0,
        tiled=True,
    )
    result = (resid.astype(jnp.float32) + down_out).astype(jnp.bfloat16)
    return (result, new_memory, new_normalizer, new_max)


def solution(mesh):
    placed = (
        P("kv", "tp"),
        P(),
        P(None, "tp"),
        P(None, "tp"),
        P(None, "tp"),
        P(None, "tp"),
        P(),
        P(),
        P("kv", "tp", None, None),
        P("kv", "tp", None),
        P("kv", "tp"),
        P(None, "tp"),
        P("tp"),
        P("tp", "kv"),
        P("tp", "kv"),
        P("kv", "tp"),
    )
    return jax.shard_map(
        per_device,
        mesh=mesh,
        in_specs=placed,
        out_specs=(P("kv", "tp"), P("kv", "tp", None, None), P("kv", "tp", None), P("kv", "tp")),
        check_vma=False,
    )
```

profile of v0, /device:TPU:0, one launch (start us, length us, event | category | flops | bytes accessed | tf_op | source)
XLA Modules:
  0.0 181.3 jit_solution(10911743880774895137)
XLA Ops:
  7.2 0.0 all-reduce.3.cloned.1.call-start
  7.3 2.3 %all_gather.9 = bf16[16,2048]{1,0:T(8,128)(2,1)S(1)} all-gather(bf16[16,1024]{1,0:T(8,128)(2,1)} %param.16), channel_id=1, replica_groups=mesh['kv'=16,'tp'=2] {'tp'}, dimensions={1}, use_global_device_ids=true | all-gather | bytes 98304 | tf_op jit(solution)/shard_map/all_gather | solution.py:35
  9.6 0.1 fusion.11
  9.8 2.0 %convolution_multiply_fusion = f32[16,512]{1,0:T(8,128)S(1)} fusion(bf16[2048,512]{1,0:T(8,128)(2,1)} %param.18, bf16[16,2048]{1,0:T(8,128)(2,1)S(1)} %all_gather.9, f32[2048]{0:T(1024)} %param.17, f32[16]{0:T(128)S(1)} %add_rsqrt_fusion.2), kind=kOutput, calls=%fused_computation.7 | convolution fusion | flops 33693696 | bytes 2203712 | tf_op jit(solution)/shard_map/dot_general | solution.py:41
  11.9 0.2 fusion.21
  12.1 0.2 fusion.23
  12.3 0.1 copy.25
  12.4 0.1 copy.26
  12.5 2.0 %fusion.19 = f32[16,512]{1,0:T(8,128)S(1)} fusion(bf16[2048,512]{1,0:T(8,128)(2,1)} %param.19, bf16[16,2048]{1,0:T(8,128)(2,1)S(1)} %all_gather.9, f32[2048]{0:T(1024)S(1)} %copy-done.3, f32[16]{0:T(128)S(1)} %add_rsqrt_fusion.2), kind=kOutput, calls=%fused_computation.43 | convolution fusion | flops 33685504 | bytes 2203712 | tf_op jit(solution)/shard_map/dot_general | solution.py:41
  14.6 0.7 multiply_reduce_fusion.1
  15.3 0.1 copy.29
  15.4 0.1 copy.30
  15.5 2.2 %fusion.17 = f32[16,512]{1,0:T(8,128)S(1)} fusion(bf16[2048,512]{1,0:T(8,128)(2,1)} %param.20, bf16[16,2048]{1,0:T(8,128)(2,1)S(1)} %all_gather.9, f32[2048]{0:T(1024)S(1)} %copy-done.3, f32[16]{0:T(128)S(1)} %add_rsqrt_fusion.2), kind=kOutput, calls=%fused_computation.42 | convolution fusion | flops 33685504 | bytes 2203712 | tf_op jit(solution)/shard_map/dot_general | solution.py:41
  17.6 0.1 copy-done.2
  17.7 0.4 fusion.3
  18.2 3.7 %multiply_add_fusion = f32[16,4,128,128]{3,2,1,0:T(8,128)S(1)} fusion(f32[16,4,128,128]{3,2,1,0:T(8,128)} %param.24, f32[16,4,128]{2,1,0:T(4,128)S(1)} %mul.143, f32[16,4,128]{2,1,0:T(4,128)S(1)} %mul.141, f32[16,4]{1,0:T(8,128)S(1)} %copy.26, f32[16,4]{1,0:T(8,128)S(1)} %copy.25), kind=kLoop, calls=%fused_computation | loop fusion | flops 4194304 | bytes 8454656 | tf_op jit(solution)/shard_map/add | solution.py:63
  21.9 3.7 %fusion.28 = f32[16,4,1,128]{3,2,1,0:T(1,128)S(1)} fusion(f32[16,4,128,1]{2,3,1,0:T(1,128)S(1)} %bitcast.20, f32[16,4,128,128]{3,2,1,0:T(8,128)S(1)} %multiply_add_fusion), kind=kOutput, calls=%fused_computation.47 | convolution fusion | flops 12582912 | bytes 4259840 | tf_op jit(solution)/shard_map/bhd,bhdv->bhv/dot_general | solution.py:67
  25.6 0.2 fusion.27
  25.8 0.2 multiply_reduce_fusion
  26.0 0.1 multiply_convert_fusion.2
  26.1 1.8 %all_gather.10 = bf16[16,1024]{1,0:T(8,128)(2,1)S(1)} all-gather(bf16[16,512]{1,0:T(8,128)(2,1)S(1)} %bitcast.22), channel_id=1, replica_groups=mesh['kv'=16,'tp'=2] {'tp'}, dimensions={1}, use_global_device_ids=true | all-gather | bytes 49152 | tf_op jit(solution)/shard_map/all_gather | solution.py:79
  27.9 0.4 fusion
  28.3 45.4 %all_gather.11 = bf16[256,1024]{1,0:T(8,128)(2,1)S(1)} all-gather(bf16[16,1024]{1,0:T(8,128)(2,1)S(1)} %fusion), channel_id=1, replica_groups=mesh['kv'=16,'tp'=2] {'kv'}, dimensions={0}, use_global_device_ids=true | all-gather | bytes 557056 | tf_op jit(solution)/shard_map/all_gather | solution.py:84
  73.7 1.1 convolution_convert_fusion
  74.8 1.1 convolution_convert_fusion.1
  75.9 0.0 reduce-scatter.2.cloned.1.call-start
  75.9 0.2 fusion.4
  76.1 2.5 %psum.21 = bf16[256]{0:T(256)(128)(2,1)S(1)} all-reduce(bf16[256]{0:T(256)(128)(2,1)S(1)} %fusion.4), channel_id=1, replica_groups=mesh['kv'=16,'tp'=2] {'tp'}, use_global_device_ids=true, to_apply=%region_5.6 | all-reduce | flops 256 | bytes 1024 | tf_op jit(solution)/shard_map/psum | solution.py:93
  78.6 11.7 %all-reduce.3.cloned.1.call-done = (bf16[256,352]{0,1:T(8,128)(2,1)}, bf16[256,352]{0,1:T(8,128)(2,1)}) async-done(((bf16[256,352]{0,1:T(8,128)(2,1)}, bf16[256,352]{0,1:T(8,128)(2,1)}), (bf16[256,352]{0,1:T(8,128)(2,1)}, bf16[256,352]{0,1:T(8,128)(2,1)})) %all-reduce.3.cloned.1.call-update) | async-done | bytes 360464 | tf_op jit(solution)/shard_map/psum | solution.py:92
  90.3 2.5 %fusion.8 = f32[256,1024]{1,0:T(8,128)} fusion(bf16[352,1024]{1,0:T(8,128)(2,1)S(1)} %copy-done.10, bf16[256,352]{0,1:T(8,128)(2,1)} %get-tuple-element.4, bf16[256,352]{0,1:T(8,128)(2,1)} %get-tuple-element.5, f32[256]{0:T(256)S(1)} %add_rsqrt_fusion.1), kind=kOutput, calls=%fused_computation.15 | convolution fusion | flops 185450496 | bytes 2130944 | tf_op jit(solution)/shard_map/dot_general | solution.py:97
  92.9 80.1 %reduce-scatter.2.cloned.1.call-done = f32[16,1024]{1,0:T(8,128)} async-done(((f32[256,1024]{1,0:T(8,128)}), f32[16,1024]{1,0:T(8,128)}) %reduce-scatter.2.cloned.1.call-update) | async-done | bytes 65552 | tf_op jit(solution)/shard_map/reduce_scatter | solution.py:96
  173.0 1.5 add_convert_fusion
  (42 shorter events, 0.3 us)
Async XLA Ops:
  7.2 20.7 %copy-start = (bf16[1024,1024]{1,0:T(8,128)(2,1)S(1)}, bf16[1024,1024]{1,0:T(8,128)(2,1)}, u32[]{:S(2)}) copy-start(bf16[1024,1024]{1,0:T(8,128)(2,1)} %param.27) | copy-start | bytes 6291460
  7.2 4.7 %copy-start.3 = (f32[2048]{0:T(1024)S(1)}, f32[2048]{0:T(1024)}, u32[]{:S(2)}) copy-start(f32[2048]{0:T(1024)} %param.17) | copy-start | bytes 24580
  7.2 4.7 %copy-start.11 = (bf16[2048,8]{0,1:T(8,128)(2,1)S(1)}, bf16[2048,8]{0,1:T(8,128)(2,1)}, u32[]{:S(2)}) copy-start(bf16[2048,8]{0,1:T(8,128)(2,1)} %param.22) | copy-start | bytes 98308
  7.2 4.9 %copy-start.12 = (bf16[2048,8]{0,1:T(8,128)(2,1)S(1)}, bf16[2048,8]{0,1:T(8,128)(2,1)}, u32[]{:S(2)}) copy-start(bf16[2048,8]{0,1:T(8,128)(2,1)} %param.23) | copy-start | bytes 98308
  7.2 5.1 %copy-start.7 = (f32[16,4]{0,1:T(4,128)S(1)}, f32[16,4]{0,1:T(4,128)}, u32[]{:S(2)}) copy-start(f32[16,4]{0,1:T(4,128)} %param.26) | copy-start | bytes 772
  7.2 83.1 %all-reduce.3.cloned.1.call-start = ((), (), s32[]{:S(2)}) async-start(), calls=%async_computation.2 | async-start | bytes 720896 | tf_op jit(solution)/shard_map/psum | solution.py:92
  9.8 4.8 %copy-start.5 = (f32[16,4,128]{2,1,0:T(4,128)S(1)}, f32[16,4,128]{2,1,0:T(4,128)}, u32[]{:S(2)}) copy-start(f32[16,4,128]{2,1,0:T(4,128)} %param.25) | copy-start | bytes 98308
  12.3 5.3 %copy-start.6 = (f32[16,4]{0,1:T(4,128)}, f32[16,4]{0,1:T(4,128)S(1)}, u32[]{:S(2)}) copy-start(f32[16,4]{0,1:T(4,128)S(1)} %get-tuple-element.11) | copy-start | bytes 772
  15.4 2.2 %copy-start.2 = (bf16[2048,512]{1,0:T(8,128)(2,1)S(1)}, bf16[2048,512]{1,0:T(8,128)(2,1)}, u32[]{:S(2)}) copy-start(bf16[2048,512]{1,0:T(8,128)(2,1)} %param.21) | copy-start | bytes 6291460
  21.9 3.7 %copy-start.1 = (f32[16,4,128,128]{3,2,1,0:T(8,128)}, f32[16,4,128,128]{3,2,1,0:T(8,128)S(1)}, u32[]{:S(2)}) copy-start(f32[16,4,128,128]{3,2,1,0:T(8,128)S(1)} %multiply_add_fusion) | copy-start | bytes 12582916
  21.9 6.0 %copy-start.4 = (bf16[16,1024]{1,0:T(8,128)(2,1)S(1)}, bf16[16,1024]{1,0:T(8,128)(2,1)}, u32[]{:S(2)}) copy-start(bf16[16,1024]{1,0:T(8,128)(2,1)} %param.16) | copy-start | bytes 98308
  25.6 48.1 %copy-start.8 = (bf16[1024,352]{0,1:T(8,128)(2,1)S(1)}, bf16[1024,352]{0,1:T(8,128)(2,1)}, u32[]{:S(2)}) copy-start(bf16[1024,352]{0,1:T(8,128)(2,1)} %param.30) | copy-start | bytes 2162692
  25.6 48.1 %copy-start.13 = (f32[1024]{0:T(1024)S(1)}, f32[1024]{0:T(1024)}, u32[]{:S(2)}) copy-start(f32[1024]{0:T(1024)} %param.28) | copy-start | bytes 12292
  27.9 46.9 %copy-start.9 = (bf16[1024,352]{0,1:T(8,128)(2,1)S(1)}, bf16[1024,352]{0,1:T(8,128)(2,1)}, u32[]{:S(2)}) copy-start(bf16[1024,352]{0,1:T(8,128)(2,1)} %param.29) | copy-start | bytes 2162692
  73.7 16.6 %copy-start.10 = (bf16[352,1024]{1,0:T(8,128)(2,1)S(1)}, bf16[352,1024]{1,0:T(8,128)(2,1)}, u32[]{:S(2)}) copy-start(bf16[352,1024]{1,0:T(8,128)(2,1)} %param.31) | copy-start | bytes 2162692
  75.9 97.1 %reduce-scatter.2.cloned.1.call-start = ((), (), s32[]{:S(2)}) async-start(), calls=%async_computation.1 | async-start | bytes 1114112 | tf_op jit(solution)/shard_map/reduce_scatter | solution.py:96
Sparse Core Ops, SparseCore 0:
  76.0 14.2 all-reduce.2
  93.0 79.9 reduce-scatter.1
where the time goes:
time: 182 us; the launch traced here: 181 us
  waiting for transfers between devices  91.8 us (50%)
  blocking collectives  52 us (29%)
  matrix products  15.8 us (9%)
  between operations  14.3 us (8%)
  other arithmetic  6.72 us (4%)
    reduce_scatter x1, waiting for transfers between devices, per_device(): lax.psum_scatter(jnp.dot(hidden, w_down, preferred_element_type=jnp.float...  80.1 us
    all_gather x1, blocking collectives, per_device(): every_row = lax.all_gather(resid, 'kv', axis=0, tiled=True)  45.4 us
    psum x1, waiting for transfers between devices, per_device(): lax.psum(up_part.astype(jnp.bfloat16), 'tp').astype(jnp.float32)  11.7 us
    dot_general x4, matrix products, project(): jnp.dot(normed, weight, preferred_element_type=jnp.float32)  6.65 us
    add x1, other arithmetic, per_device(): keep_weight[..., None, None] * memory  3.72 us
    dot_general x1, matrix products, per_device(): jnp.einsum('bhd,bhdv->bhv', queries, new_memory, precision=lax.Precision....  3.66 us
  transfers between devices with their start and end apart: 2, of which 2 were waited for; matrix products, arithmetic and copies ran while one was open for 0% of the time, Pallas kernels for 0%

commit v1 on v0

--- a/solution.py
+++ b/solution.py
@@ -1,17 +1,228 @@
+import functools
+
 import jax
 import jax.numpy as jnp
 from jax import lax
+from jax.experimental import pallas as pl
+from jax.experimental.pallas import tpu as pltpu
 from jax.sharding import PartitionSpec as P
 
-D = 2048
-
-
-def activate(gate_sum, up_sum, square_sum):
-    ffn_scale = lax.rsqrt(square_sum / D + 1e-06)[:, None]
-    return (jax.nn.silu(ffn_scale * gate_sum) * (ffn_scale * up_sum)).astype(jnp.bfloat16)
+F32, BF16 = jnp.float32, jnp.bfloat16
+MESH = pl.DeviceIdType.MESH
+ANY = pl.BlockSpec(memory_space=pl.ANY)
+VMEM = pl.BlockSpec(memory_space=pltpu.VMEM)
+
+
+def partner(index, bits):
+    out, bit = index, 1
+    while bit <= bits:
+        if bits & bit:
+            out = out + bit - 2 * bit * ((index // bit) % 2)
+        bit *= 2
+    return out
+
+
+def split_groups(count):
+    slow = 1
+    while slow * slow < count:
+        slow *= 2
+    assert count % slow == 0
+    return slow, count // slow
+
+
+def greet(devices):
+    barrier = pltpu.get_barrier_semaphore()
+    for device in devices:
+        pl.semaphore_signal(barrier, inc=1, device_id=device, device_id_type=MESH)
+    pl.semaphore_wait(barrier, len(devices))
+
+
+def mixer_kernel(
+    nz, ny, nt, width,
+    mixed_ref, tokens_ref, gain_ref, w_out_hbm, w_gate_hbm, w_up_hbm, w_down_hbm,
+    out_ref,
+    w_out, w_gate, w_up, w_down, mix, rows, part, part_in, down, down_in, total, total_in,
+    load_sem, mix_sem, zed_sem, plane_sem, part_sem, down_sem, total_sem,
+):
+    k, t = lax.axis_index("kv"), lax.axis_index("tp")
+    z, y = k // ny, k % ny
+    own, cols = rows.shape[1], rows.shape[2]
+    ff = w_down.shape[0]
+    pad = (part.shape[2] - 128) // 2
+
+    loads = [
+        pltpu.make_async_copy(src, dst, load_sem.at[i])
+        for i, (src, dst) in enumerate(
+            ((w_out_hbm, w_out), (w_gate_hbm, w_gate), (w_up_hbm, w_up), (w_down_hbm, w_down))
+        )
+    ]
+    for load in loads:
+        load.start()
+
+    def at_zed(off):
+        return (partner(z, off) * ny + y, t)
+
+    def at_plane(off):
+        return (z * ny + partner(y, off), t)
+
+    def at_tp(off):
+        return (k, partner(t, off))
+
+    greet(
+        [at_tp(o) for o in range(1, nt)]
+        + [at_plane(o) for o in range(1, ny)]
+        + [at_zed(o) for o in range(1, nz)]
+    )
+    started = []
+
+    def send(src, dst, sems, device):
+        copy = pltpu.make_async_remote_copy(
+            src_ref=src, dst_ref=dst, send_sem=sems.at[0], recv_sem=sems.at[1],
+            device_id=device, device_id_type=MESH,
+        )
+        copy.start()
+        started.append(copy)
+        return copy
+
+    mixes = [send(mixed_ref, mix.at[o - 1], mix_sem.at[o - 1], at_tp(o)) for o in range(1, nt)]
+    loads[0].wait()
+    inner = mixed_ref.shape[1]
+
+    def project(value, owner):
+        return jnp.dot(value, w_out[pl.ds(pl.multiple_of(owner * inner, inner), inner), :], preferred_element_type=F32)
+
+    acc = tokens_ref[...].astype(F32) + project(mixed_ref[...], t)
+    for o in range(1, nt):
+        mixes[o - 1].wait_recv()
+        acc = acc + project(mix[o - 1], partner(t, o))
+    resid = acc.astype(BF16)
+    rows[k] = resid
+
+    zeds = {o: send(rows.at[k], rows.at[k], zed_sem.at[o], at_zed(o)) for o in range(1, nz)}
+    planes = {}
+
+    def spread(off):
+        source = partner(z, off) * ny + y
+        if off:
+            zeds[off].wait_recv()
+        for o in range(1, ny):
+            planes[off, o] = send(rows.at[source], rows.at[source], plane_sem.at[off, o], at_plane(o))
+
+    parts, gates, downs, totals, keep = {}, {}, {}, {}, {}
+
+    def stage_a(off):
+        for o in range(1, ny):
+            planes[off, o].wait_recv()
+        if off == 0:
+            for load in loads[1:3]:
+                load.wait()
+        x = rows[pl.ds(partner(z, off) * ny, ny)].reshape(ny * own, cols)
+        xf = x.astype(F32)
+        square = jnp.sum(xf * xf, axis=-1, keepdims=True)
+        h = (xf * gain_ref[...]).astype(BF16)
+        gate = jnp.dot(h, w_gate[...], preferred_element_type=F32)
+        up = jnp.dot(h, w_up[...], preferred_element_type=F32)
+        high = square.astype(BF16).astype(F32)
+        lane = lax.broadcasted_iota(jnp.int32, (ny * own, 128), 1)
+        part[off, :, 0:ff] = gate.astype(BF16)
+        part[off, :, pad : pad + ff] = up.astype(BF16)
+        part[off, :, 2 * pad :] = jnp.where(lane < 64, high, square - high).astype(BF16)
+        for o in range(1, nt):
+            parts[off, o] = send(part.at[off], part_in.at[off, o - 1], part_sem.at[off, o - 1], at_tp(o))
+        gates[off] = (gate, up, square)
+
+    def stage_b(off):
+        gate, up, square = gates.pop(off)
+        for o in range(1, nt):
+            parts[off, o].wait_recv()
+            gate = gate + part_in[off, o - 1, :, 0:ff].astype(F32)
+            up = up + part_in[off, o - 1, :, pad : pad + ff].astype(F32)
+            tail = part_in[off, o - 1, :, 2 * pad :].astype(F32)
+            square = square + jnp.sum(tail, axis=-1, keepdims=True) * (1.0 / 64)
+        scale = lax.rsqrt(square / width + 1e-06)
+        g = scale * gate
+        hidden = (g / (1.0 + jnp.exp(-g)) * (scale * up)).astype(BF16)
+        if off == 0:
+            loads[3].wait()
+        out = jnp.dot(hidden, w_down[...], preferred_element_type=F32)
+        down[off] = out.reshape(ny, own, cols).astype(BF16)
+        for o in range(1, ny):
+            downs[off, o] = send(down.at[off, partner(y, o)], down_in.at[off, o - 1], down_sem.at[off, o], at_plane(o))
+
+    def stage_c(off):
+        acc = down[off, y].astype(F32)
+        for o in range(1, ny):
+            downs[off, o].wait_recv()
+            acc = acc + down_in[off, o - 1].astype(F32)
+        if off == 0:
+            keep[0] = acc
+        else:
+            total[off] = acc.astype(BF16)
+            totals[off] = send(total.at[off], total_in.at[off], total_sem.at[off], at_zed(off))
+
+    spread(0)
+    if nz > 1:
+        spread(1)
+    stage_a(0)
+    for o in range(2, nz):
+        spread(o)
+    for o in range(0, nz + 2):
+        if 1 <= o + 1 < nz:
+            stage_a(o + 1)
+        if o < nz:
+            stage_b(o)
+        if 0 <= o - 1 < nz:
+            stage_c(o - 1)
+    acc = rows[k].astype(F32) + keep[0]
+    for o in range(1, nz):
+        totals[o].wait_recv()
+        acc = acc + total_in[o].astype(F32)
+    out_ref[...] = acc.astype(BF16)
+    for copy in started:
+        copy.wait_send()
+
+
+def channel_mixer(mesh, mixed, tokens, ffn_gain, w_output, w_gate, w_up, w_down):
+    n, nt = mesh.shape["kv"], mesh.shape["tp"]
+    nz, ny = split_groups(n)
+    own, cols = tokens.shape
+    ff = w_down.shape[0]
+    pad = -(-ff // 128) * 128
+    dma = pltpu.SemaphoreType.DMA
+    peers = max(nt - 1, 1)
+    return pl.pallas_call(
+        functools.partial(mixer_kernel, nz, ny, nt, cols * nt),
+        out_shape=jax.ShapeDtypeStruct((own, cols), BF16),
+        in_specs=[VMEM, VMEM, VMEM, ANY, ANY, ANY, ANY],
+        out_specs=VMEM,
+        scratch_shapes=[
+            pltpu.VMEM(w_output.shape, BF16),
+            pltpu.VMEM(w_gate.shape, BF16),
+            pltpu.VMEM(w_up.shape, BF16),
+            pltpu.VMEM(w_down.shape, BF16),
+            pltpu.VMEM((peers,) + mixed.shape, BF16),
+            pltpu.VMEM((n, own, cols), BF16),
+            pltpu.VMEM((nz, ny * own, 2 * pad + 128), BF16),
+            pltpu.VMEM((nz, peers, ny * own, 2 * pad + 128), BF16),
+            pltpu.VMEM((nz, ny, own, cols), BF16),
+            pltpu.VMEM((nz, ny, own, cols), BF16),
+            pltpu.VMEM((nz, own, cols), BF16),
+            pltpu.VMEM((nz, own, cols), BF16),
+            dma((4,)),
+            dma((peers, 2)),
+            dma((nz, 2)),
+            dma((nz, ny, 2)),
+            dma((nz, peers, 2)),
+            dma((nz, ny, 2)),
+            dma((nz, 2)),
+        ],
+        compiler_params=pltpu.CompilerParams(collective_id=0, has_side_effects=True),
+        name="channel_mixer",
+    )(mixed, tokens, ffn_gain.reshape(1, cols), w_output, w_gate, w_up, w_down)
 
 
 def per_device(
+    mesh,
     tokens,
     norm_gain,
     w_query,
@@ -75,31 +286,7 @@
         .reshape(local_rows, head_count * head_dim)
         .astype(jnp.bfloat16)
     )
-    branch_out = jnp.dot(
-        lax.all_gather(mixed, "tp", axis=1, tiled=True),
-        w_output,
-        preferred_element_type=jnp.float32,
-    )
-    resid = (tokens.astype(jnp.float32) + branch_out).astype(jnp.bfloat16)
-    every_row = lax.all_gather(resid, "kv", axis=0, tiled=True)
-    every_f = every_row.astype(jnp.float32)
-    square_part = jnp.sum(every_f * every_f, axis=-1)
-    ffn_in = (every_f * ffn_gain).astype(jnp.bfloat16)
-    gate_part = jnp.dot(ffn_in, w_gate, preferred_element_type=jnp.float32)
-    up_part = jnp.dot(ffn_in, w_up, preferred_element_type=jnp.float32)
-    gate_full, up_full, square_full = (
-        lax.psum(gate_part.astype(jnp.bfloat16), "tp").astype(jnp.float32),
-        lax.psum(up_part.astype(jnp.bfloat16), "tp").astype(jnp.float32),
-        lax.psum(square_part.astype(jnp.bfloat16), "tp").astype(jnp.float32),
-    )
-    hidden = activate(gate_full, up_full, square_full)
-    down_out = lax.psum_scatter(
-        jnp.dot(hidden, w_down, preferred_element_type=jnp.float32),
-        "kv",
-        scatter_dimension=0,
-        tiled=True,
-    )
-    result = (resid.astype(jnp.float32) + down_out).astype(jnp.bfloat16)
+    result = channel_mixer(mesh, mixed, tokens, ffn_gain, w_output, w_gate, w_up, w_down)
     return (result, new_memory, new_normalizer, new_max)
 
 
@@ -123,7 +310,7 @@
         P("kv", "tp"),
     )
     return jax.shard_map(
-        per_device,
+        functools.partial(per_device, mesh),
         mesh=mesh,
         in_specs=placed,
         out_specs=(P("kv", "tp"), P("kv", "tp", None, None), P("kv", "tp", None), P("kv", "tp")),

time: 182 us -> 59.2 us (0.33)
  waiting for transfers between devices: 91.8 us -> 0 us
  blocking collectives: 52 us -> 2.34 us
  Pallas kernels: 0 us -> 30 us
  between operations: 14.3 us -> 0.79 us
  local copies, waits for them, and re-layouts: 0.54 us -> 5.88 us
  matrix products: 15.8 us -> 12.8 us
    reduce_scatter x1 -> x0, waiting for transfers between devices: 80.1 us -> none  [per_device(): lax.psum_scatter(jnp.dot(hidden, w_down, preferred_element_type=jnp.float...]
    all_gather x2 -> x0, blocking collectives: 47.2 us -> none  [the longest x1 45.4 us: per_device(): every_row = lax.all_gather(resid, 'kv', axis=0, tiled=True)]
    pallas_call x0 -> x1, Pallas kernels: none -> 30 us  [channel_mixer(): pl.pallas_call(functools.partial(mixer_kernel, nz, ny, nt, cols * nt), ou...]
    psum x1 -> x0, waiting for transfers between devices: 11.7 us -> none  [per_device(): lax.psum(up_part.astype(jnp.bfloat16), 'tp').astype(jnp.float32)]
    unnamed x29 -> x16, local copies, waits for them, and re-layouts: 0.13 us -> 5.46 us
    dot_general x4 -> x0, matrix products: 5.06 us -> none  [the longest x1 2.54 us: per_device(): jnp.dot(hidden, w_down, preferred_element_type=jnp.float32)]
    psum x1 -> x0, blocking collectives: 2.47 us -> none  [per_device(): lax.psum(square_part.astype(jnp.bfloat16), 'tp').astype(jnp.float32)]
  transfers between devices with their start and end apart: 2 -> 0, of which waited for: 2 -> 0; matrix products, arithmetic and copies ran while one was open for 0% -> 0% of each run, Pallas kernels for 0% -> 0%
where the time goes in v1:
time: 59.2 us; the launch traced here: 58.6 us
  Pallas kernels  30 us (51%)
  matrix products  12.8 us (22%)
  other arithmetic  6.76 us (11%)
  local copies, waits for them, and re-layouts  5.88 us (10%)
  blocking collectives  2.34 us (4%)
  between operations  0.79 us (1%)
    pallas_call x1, Pallas kernels, channel_mixer(): pl.pallas_call(functools.partial(mixer_kernel, nz, ny, nt, cols * nt), ou...  30 us
    dot_general x4, matrix products, project(): jnp.dot(normed, weight, preferred_element_type=jnp.float32)  5.58 us
    unnamed x16, local copies, waits for them, and re-layouts  5.46 us
    dot_general x1, matrix products, per_device(): jnp.einsum('bhd,bhdv->bhv', queries, new_memory, precision=lax.Precision....  5.28 us
    add x1, other arithmetic, per_device(): keep_weight[..., None, None] * memory  4.73 us
    all_gather x1, blocking collectives, per_device(): full_rows = lax.all_gather(tokens, 'tp', axis=1, tiled=True)  2.34 us

profile of v1, /device:TPU:0, one launch (start us, length us, event | category | flops | bytes accessed | tf_op | source)
XLA Modules:
  0.0 58.6 jit_solution(1122576249521290888)
XLA Ops:
  0.6 0.0 copy-start
  0.6 0.0 copy-start.3
  0.7 2.3 %all_gather.3 = bf16[16,2048]{1,0:T(8,128)(2,1)S(1)} all-gather(bf16[16,1024]{1,0:T(8,128)(2,1)} %tokens_ref.1), channel_id=1, replica_groups=mesh['kv'=16,'tp'=2] {'tp'}, dimensions={1}, use_global_device_ids=true | all-gather | bytes 98304 | tf_op jit(solution)/shard_map/all_gather | solution.py:246
  3.0 0.1 fusion.3
  3.1 1.0 %fusion.12 = f32[16,8]{0,1:T(8,128)S(1)} fusion(bf16[2048,8]{0,1:T(8,128)(2,1)} %param.22, bf16[16,2048]{1,0:T(8,128)(2,1)S(1)} %all_gather.3, f32[2048]{0:T(1024)} %param.17, f32[16]{0:T(128)S(1)} %add_rsqrt_fusion.1), kind=kOutput, calls=%fused_computation.29 | convolution fusion | flops 655360 | bytes 107072 | tf_op jit(solution)/shard_map/dot_general | solution.py:262
  4.1 1.0 %fusion.14 = f32[16,8]{0,1:T(8,128)S(1)} fusion(bf16[2048,8]{0,1:T(8,128)(2,1)} %param.23, bf16[16,2048]{1,0:T(8,128)(2,1)S(1)} %all_gather.3, f32[2048]{0:T(1024)} %param.17, f32[16]{0:T(128)S(1)} %add_rsqrt_fusion.1), kind=kOutput, calls=%fused_computation.30 | convolution fusion | flops 655360 | bytes 107072 | tf_op jit(solution)/shard_map/dot_general | solution.py:265
  5.1 0.7 %subtract_exponential_fusion.1 = (f32[16,4]{0,1:T(4,128)S(1)}, f32[16,4]{0,1:T(4,128)S(1)}) fusion(f32[16,4]{0,1:T(4,128)} %param.26, f32[16,8]{0,1:T(8,128)S(1)} %fusion.14, s32[]{:T(128)S(6)} %select_n.9, f32[16,8]{0,1:T(8,128)S(1)} %fusion.12), kind=kLoop, calls=%fused_computation.24 | loop fusion | flops 704 | bytes 1284 | tf_op jit(solution)/shard_map/exp | solution.py:272
  5.8 0.0 copy-start.5
  5.8 0.1 copy.28
  5.9 0.1 copy.27
  6.0 0.0 copy-done
  6.0 1.1 %fusion.10 = f32[16,512]{1,0:T(8,128)S(1)} fusion(bf16[2048,512]{1,0:T(8,128)(2,1)S(1)} %copy-done, bf16[16,2048]{1,0:T(8,128)(2,1)S(1)} %all_gather.3, f32[2048]{0:T(1024)} %param.17, f32[16]{0:T(128)S(1)} %add_rsqrt_fusion.1), kind=kOutput, calls=%fused_computation.28 | convolution fusion | flops 33685504 | bytes 2203712 | tf_op jit(solution)/shard_map/dot_general | solution.py:252
  7.1 0.0 copy-done.3
  7.2 2.0 %fusion.8 = f32[16,512]{1,0:T(8,128)S(1)} fusion(bf16[2048,512]{1,0:T(8,128)(2,1)} %param.20, bf16[16,2048]{1,0:T(8,128)(2,1)S(1)} %all_gather.3, f32[2048]{0:T(1024)S(1)} %copy-done.3, f32[16]{0:T(128)S(1)} %add_rsqrt_fusion.1), kind=kOutput, calls=%fused_computation.27 | convolution fusion | flops 33685504 | bytes 2203712 | tf_op jit(solution)/shard_map/dot_general | solution.py:252
  9.2 0.0 copy-start.1
  9.2 4.7 %multiply_add_fusion = f32[16,4,128,128]{3,2,1,0:T(8,128)} fusion(f32[16,4,128,128]{3,2,1,0:T(8,128)} %param.24, f32[16,4,128]{2,1,0:T(4,128)S(1)} %mul.111, f32[16,4,128]{2,1,0:T(4,128)S(1)} %mul.109, f32[16,4]{1,0:T(8,128)S(1)} %copy.28, f32[16,4]{1,0:T(8,128)S(1)} %copy.27), kind=kLoop, calls=%fused_computation | loop fusion | flops 4194304 | bytes 8454656 | tf_op jit(solution)/shard_map/add | solution.py:274
  13.9 0.0 copy-done.1
  13.9 0.4 convolution_multiply_fusion
  14.4 0.0 copy-start.4
  14.4 5.3 %fusion.19 = f32[16,4,1,128]{3,2,1,0:T(1,128)S(1)} fusion(f32[16,4,128,1]{2,3,1,0:T(1,128)S(1)} %bitcast.17, f32[16,4,128,128]{3,2,1,0:T(8,128)} %multiply_add_fusion), kind=kOutput, calls=%fused_computation.32 | convolution fusion | flops 12582912 | bytes 4259840 | tf_op jit(solution)/shard_map/bhd,bhdv->bhv/dot_general | solution.py:278
  19.7 0.7 %multiply_reduce_fusion.1 = (f32[16,4]{1,0:T(8,128)S(1)}, f32[16,4,128]{2,1,0:T(4,128)}) fusion(f32[16,4,128]{2,1,0:T(4,128)S(1)} %mul.104, f32[16,4,128]{2,1,0:T(4,128)S(1)} %mul.109, f32[16,4]{1,0:T(8,128)S(1)} %copy.28, f32[16,4,128]{2,1,0:T(4,128)S(1)} %copy-done.4, f32[16,4]{1,0:T(8,128)S(1)} %copy.27), kind=kLoop, calls=%fused_computation.13 | loop fusion | flops 40896 | bytes 131840 | tf_op jit(solution)/shard_map/reduce_sum | solution.py:279
  20.4 0.1 copy.31
  20.5 0.1 copy.32
  20.6 0.2 fusion.18
  20.8 0.2 multiply_reduce_fusion
  21.0 2.0 %fusion.2 = f32[16,512]{1,0:T(8,128)S(1)} fusion(bf16[2048,512]{1,0:T(8,128)(2,1)} %param.21, bf16[16,2048]{1,0:T(8,128)(2,1)S(1)} %all_gather.3, f32[2048]{0:T(1024)S(1)} %copy-done.3, f32[16]{0:T(128)S(1)} %add_rsqrt_fusion.1), kind=kOutput, calls=%fused_computation.5 | convolution fusion | flops 33710080 | bytes 2203712 | tf_op jit(solution)/shard_map/dot_general | solution.py:252
  23.0 0.1 multiply_convert_fusion
  23.1 0.6 %copy.39 = bf16[2,8,4,128]{3,1,2,0:T(8,128)(2,1)} copy(bf16[2,8,4,128]{3,2,1,0:T(4,128)(2,1)S(1)} %bitcast.19) | data formatting | bytes 32768
  23.8 1.2 %copy.33.w_gate_hbm = bf16[1024,352]{1,0:T(8,128)(2,1)} copy(bf16[1024,352]{0,1:T(8,128)(2,1)S(1)} %copy-done.2) | data formatting | bytes 1441792 | tf_op args[13]
  24.9 2.3 %copy.34.w_up_hbm = bf16[1024,352]{1,0:T(8,128)(2,1)} copy(bf16[1024,352]{0,1:T(8,128)(2,1)} %param.30) | data formatting | bytes 1441792 | tf_op args[14]
  27.2 30.0 %channel_mixer.1 = bf16[16,1024]{1,0:T(8,128)(2,1)} custom-call(bf16[16,512]{1,0:T(8,128)(2,1)} %bitcast.18, bf16[16,1024]{1,0:T(8,128)(2,1)} %tokens_ref.1, f32[1,1024]{1,0:T(1,128)} %bitcast.20, bf16[1024,1024]{1,0:T(8,128)(2,1)} %w_out_hbm.1, bf16[1024,352]{1,0:T(8,128)(2,1)} %copy.33.w_gate_hbm, bf16[1024,352]{1,0:T(8,128)(2,1)} %copy.34.w_up_hbm, ...), custom_call_target="tpu_custom_call" | custom-call | tf_op jit(solution)/shard_map/channel_mixer/pallas_call | solution.py:193
  57.2 1.4 %copy.41 = bf16[16,1024]{1,0:T(8,128)(2,1)} copy(bf16[16,1024]{1,0:T(8,128)(2,1)} %channel_mixer.1) | data formatting | bytes 65536
  (14 shorter events, 0.1 us)
Async XLA Ops:
  0.6 5.4 %copy-start = (bf16[2048,512]{1,0:T(8,128)(2,1)S(1)}, bf16[2048,512]{1,0:T(8,128)(2,1)}, u32[]{:S(2)}) copy-start(bf16[2048,512]{1,0:T(8,128)(2,1)} %param.19) | copy-start | bytes 6291460
  0.6 6.5 %copy-start.3 = (f32[2048]{0:T(1024)S(1)}, f32[2048]{0:T(1024)}, u32[]{:S(2)}) copy-start(f32[2048]{0:T(1024)} %param.17) | copy-start | bytes 24580
  5.8 14.7 %copy-start.5 = (f32[16,4]{0,1:T(4,128)}, f32[16,4]{0,1:T(4,128)S(1)}, u32[]{:S(2)}) copy-start(f32[16,4]{0,1:T(4,128)S(1)} %get-tuple-element.17) | copy-start | bytes 772
  9.2 4.7 %copy-start.1 = (bf16[2048,512]{1,0:T(8,128)(2,1)S(1)}, bf16[2048,512]{1,0:T(8,128)(2,1)}, u32[]{:S(2)}) copy-start(bf16[2048,512]{1,0:T(8,128)(2,1)} %param.18) | copy-start | bytes 6291460
  14.4 5.3 %copy-start.4 = (f32[16,4,128]{2,1,0:T(4,128)S(1)}, f32[16,4,128]{2,1,0:T(4,128)}, u32[]{:S(2)}) copy-start(f32[16,4,128]{2,1,0:T(4,128)} %param.25) | copy-start | bytes 98308
  19.7 4.1 %copy-start.2 = (bf16[1024,352]{0,1:T(8,128)(2,1)S(1)}, bf16[1024,352]{0,1:T(8,128)(2,1)}, u32[]{:S(2)}) copy-start(bf16[1024,352]{0,1:T(8,128)(2,1)} %param.29) | copy-start | bytes 2162692

commit v2 on v1

v2 whole, which is shorter than its diff:
```python
import functools

import jax
import jax.numpy as jnp
from jax import lax
from jax.experimental import pallas as pl
from jax.experimental.pallas import tpu as pltpu
from jax.sharding import PartitionSpec as P

F32, BF16 = jnp.float32, jnp.bfloat16
MESH = pl.DeviceIdType.MESH
ANY = pl.BlockSpec(memory_space=pl.ANY)
VMEM = pl.BlockSpec(memory_space=pltpu.VMEM)
DEPTH = 4


def partner(index, bits):
    out, bit = index, 1
    while bit <= bits:
        if bits & bit:
            out = out + bit - 2 * bit * ((index // bit) % 2)
        bit *= 2
    return out


def split_groups(count):
    slow = 1
    while slow * slow < count:
        slow *= 2
    assert count % slow == 0
    return slow, count // slow


def greet(devices):
    barrier = pltpu.get_barrier_semaphore()
    for device in devices:
        pl.semaphore_signal(barrier, inc=1, device_id=device, device_id_type=MESH)
    pl.semaphore_wait(barrier, len(devices))


def nt_dot(a, b):
    return lax.dot_general(a, b, (((1,), (1,)), ((), ())), preferred_element_type=F32)


def step_kernel(
    nz, ny, nt, width,
    tokens_ref, norm_gain_ref, w_ig_ref, w_fg_ref, normalizer_ref, memory_max_ref, gain_ref,
    w_key_hbm, w_value_hbm, w_query_hbm, w_outgate_hbm, memory_hbm, w_out_hbm, w_gate_hbm, w_up_hbm, w_down_hbm,
    out_ref, aux_ref, new_max_ref,
    w_key, w_value, w_query, w_outgate, memory, w_out, w_gate, w_up, w_down,
    tok, normed, num, mixed_ref, mix, rows, part, part_in, down, down_in, total, total_in,
    load_sem, tok_sem, mix_sem, zed_sem, plane_sem, part_sem, down_sem, total_sem,
):
    k, t = lax.axis_index("kv"), lax.axis_index("tp")
    z, y = k // ny, k % ny
    own, cols = rows.shape[1], rows.shape[2]
    heads, dim = memory.shape[0], memory.shape[3]
    ff = w_down.shape[0]
    pad = (part.shape[2] - 128) // 2

    pairs = [(w_key_hbm, w_key), (w_value_hbm, w_value), (w_query_hbm, w_query), (w_outgate_hbm, w_outgate)]
    pairs += [(memory_hbm.at[:, h], memory.at[h]) for h in range(heads)]
    pairs += [(w_out_hbm, w_out), (w_gate_hbm, w_gate), (w_up_hbm, w_up), (w_down_hbm, w_down)]
    loads = [pltpu.make_async_copy(src, dst, load_sem.at[i]) for i, (src, dst) in enumerate(pairs)]
    for load in loads[:DEPTH]:
        load.start()

    def arrived(i):
        loads[i].wait()
        if i + DEPTH < len(loads):
            loads[i + DEPTH].start()

    def at_zed(off):
        return (partner(z, off) * ny + y, t)

    def at_plane(off):
        return (z * ny + partner(y, off), t)

    def at_tp(off):
        return (k, partner(t, off))

    greet(
        [at_tp(o) for o in range(1, nt)]
        + [at_plane(o) for o in range(1, ny)]
        + [at_zed(o) for o in range(1, nz)]
    )
    started = []

    def send(src, dst, sems, device):
        copy = pltpu.make_async_remote_copy(
            src_ref=src, dst_ref=dst, send_sem=sems.at[0], recv_sem=sems.at[1],
            device_id=device, device_id_type=MESH,
        )
        copy.start()
        started.append(copy)
        return copy

    toks = [send(tokens_ref, tok.at[o - 1], tok_sem.at[o - 1], at_tp(o)) for o in range(1, nt)]
    blocks = [(t, tokens_ref[...].astype(F32))]
    for o in range(1, nt):
        toks[o - 1].wait_recv()
        blocks.append((partner(t, o), tok[o - 1].astype(F32)))
    square = blocks[0][1] * blocks[0][1]
    square = jnp.sum(square, axis=-1, keepdims=True)
    for _, block in blocks[1:]:
        square = square + jnp.sum(block * block, axis=-1, keepdims=True)
    row_scale = lax.rsqrt(square / width + 1e-06)
    for owner, block in blocks:
        at = pl.ds(pl.multiple_of(owner * cols, cols), cols)
        normed[:, at] = (block * row_scale * norm_gain_ref[:, at]).astype(BF16)
    x = normed[...]
    igates, fgates = nt_dot(x, w_ig_ref[...]), nt_dot(x, w_fg_ref[...])

    def projected(i, weight):
        arrived(i)
        return jnp.dot(x, weight[...], preferred_element_type=F32)

    keys = projected(0, w_key)
    values = projected(1, w_value)
    queries = projected(2, w_query) * dim ** (-0.5)
    outgates = projected(3, w_outgate)
    lane = lax.broadcasted_iota(jnp.int32, igates.shape, 1)
    for h in range(heads):
        mine = lane == t * heads + h
        igate = jnp.sum(jnp.where(mine, igates, 0.0), axis=-1, keepdims=True)
        forget = jnp.sum(jnp.where(mine, fgates, 0.0), axis=-1, keepdims=True)
        carried = jnp.minimum(forget, 0.0) - jnp.log1p(jnp.exp(-jnp.abs(forget))) + memory_max_ref[:, h : h + 1]
        new_max = jnp.maximum(carried, igate)
        keep_weight = jnp.exp(carried - new_max)
        new_max_ref[:, h : h + 1] = new_max
        at = slice(h * dim, (h + 1) * dim)
        key, value, query = jnp.exp(igate - new_max) * keys[:, at], values[:, at], queries[:, at]
        keep_wide = jnp.broadcast_to(keep_weight, key.shape)
        aux_ref[0, h], aux_ref[1, h], aux_ref[2, h] = keep_wide, key, value
        denominator = jnp.sum(query * (keep_wide * normalizer_ref[:, h, :] + key), axis=-1, keepdims=True)
        match = jnp.sum(query * key, axis=-1, keepdims=True)
        turned = query.T
        arrived(4 + h)
        for r in range(own):
            num[r : r + 1, :] = jnp.sum(memory[h, r] * turned[:, r : r + 1], axis=0, keepdims=True)
        numerator = keep_wide * num[...] + match * value
        cell_out = numerator / jnp.maximum(jnp.abs(denominator), jnp.exp(-new_max))
        centered = cell_out - jnp.mean(cell_out, axis=-1, keepdims=True)
        head_var = jnp.mean(centered * centered, axis=-1, keepdims=True)
        gate = 1.0 / (1.0 + jnp.exp(-outgates[:, at]))
        mixed_ref[:, at] = (gate * centered * lax.rsqrt(head_var + 1e-05)).astype(BF16)

    mixes = [send(mixed_ref, mix.at[o - 1], mix_sem.at[o - 1], at_tp(o)) for o in range(1, nt)]
    first = 4 + heads
    arrived(first)
    inner = mixed_ref.shape[1]

    def project(value, owner):
        return jnp.dot(value, w_out[pl.ds(pl.multiple_of(owner * inner, inner), inner), :], preferred_element_type=F32)

    acc = tokens_ref[...].astype(F32) + project(mixed_ref[...], t)
    for o in range(1, nt):
        mixes[o - 1].wait_recv()
        acc = acc + project(mix[o - 1], partner(t, o))
    rows[k] = acc.astype(BF16)

    zeds = {o: send(rows.at[k], rows.at[k], zed_sem.at[o], at_zed(o)) for o in range(1, nz)}
    planes = {}

    def spread(off):
        source = partner(z, off) * ny + y
        if off:
            zeds[off].wait_recv()
        for o in range(1, ny):
            planes[off, o] = send(rows.at[source], rows.at[source], plane_sem.at[off, o], at_plane(o))

    parts, gates, downs, totals, keep = {}, {}, {}, {}, {}

    def stage_a(off):
        for o in range(1, ny):
            planes[off, o].wait_recv()
        if off == 0:
            arrived(first + 1)
            arrived(first + 2)
        x = rows[pl.ds(partner(z, off) * ny, ny)].reshape(ny * own, cols)
        xf = x.astype(F32)
        square = jnp.sum(xf * xf, axis=-1, keepdims=True)
        h = (xf * gain_ref[...]).astype(BF16)
        gate = nt_dot(h, w_gate[...])
        up = nt_dot(h, w_up[...])
        high = square.astype(BF16).astype(F32)
        lane = lax.broadcasted_iota(jnp.int32, (ny * own, 128), 1)
        part[off, :, 0:ff] = gate.astype(BF16)
        part[off, :, pad : pad + ff] = up.astype(BF16)
        part[off, :, 2 * pad :] = jnp.where(lane < 64, high, square - high).astype(BF16)
        for o in range(1, nt):
            parts[off, o] = send(part.at[off], part_in.at[off, o - 1], part_sem.at[off, o - 1], at_tp(o))
        gates[off] = (gate, up, square)

    def stage_b(off):
        gate, up, square = gates.pop(off)
        for o in range(1, nt):
            parts[off, o].wait_recv()
            gate = gate + part_in[off, o - 1, :, 0:ff].astype(F32)
            up = up + part_in[off, o - 1, :, pad : pad + ff].astype(F32)
            tail = part_in[off, o - 1, :, 2 * pad :].astype(F32)
            square = square + jnp.sum(tail, axis=-1, keepdims=True) * (1.0 / 64)
        scale = lax.rsqrt(square / width + 1e-06)
        g = scale * gate
        hidden = (g / (1.0 + jnp.exp(-g)) * (scale * up)).astype(BF16)
        if off == 0:
            arrived(first + 3)
        out = jnp.dot(hidden, w_down[...], preferred_element_type=F32)
        down[off] = out.reshape(ny, own, cols).astype(BF16)
        for o in range(1, ny):
            downs[off, o] = send(down.at[off, partner(y, o)], down_in.at[off, o - 1], down_sem.at[off, o], at_plane(o))

    def stage_c(off):
        acc = down[off, y].astype(F32)
        for o in range(1, ny):
            downs[off, o].wait_recv()
            acc = acc + down_in[off, o - 1].astype(F32)
        if off == 0:
            keep[0] = acc
        else:
            total[off] = acc.astype(BF16)
            totals[off] = send(total.at[off], total_in.at[off], total_sem.at[off], at_zed(off))

    spread(0)
    if nz > 1:
        spread(1)
    stage_a(0)
    for o in range(2, nz):
        spread(o)
    for o in range(0, nz + 2):
        if 1 <= o + 1 < nz:
            stage_a(o + 1)
        if o < nz:
            stage_b(o)
        if 0 <= o - 1 < nz:
            stage_c(o - 1)
    acc = rows[k].astype(F32) + keep[0]
    for o in range(1, nz):
        totals[o].wait_recv()
        acc = acc + total_in[o].astype(F32)
    out_ref[...] = acc.astype(BF16)
    for copy in started:
        copy.wait_send()


def update_kernel(chunk, memory_hbm, aux_ref, normalizer_ref, new_max_in, result_in, new_memory_hbm, new_norm_ref, new_max_ref, result_ref, memory, in_sem, out_sem):
    rows, heads = memory.shape[0], memory.shape[1]
    steps = range(rows // chunk)
    at = [pl.ds(i * chunk, chunk) for i in steps]
    loads = [pltpu.make_async_copy(memory_hbm.at[at[i]], memory.at[at[i]], in_sem.at[i]) for i in steps]
    stores = [pltpu.make_async_copy(memory.at[at[i]], new_memory_hbm.at[at[i]], out_sem.at[i]) for i in steps]
    for load in loads:
        load.start()
    turned = []
    for h in range(heads):
        new_norm_ref[:, h, :] = aux_ref[0, h] * normalizer_ref[:, h, :] + aux_ref[1, h]
        turned.append(aux_ref[1, h].T)
    new_max_ref[...] = new_max_in[...]
    result_ref[...] = result_in[...]
    for i in steps:
        loads[i].wait()
        for r in range(i * chunk, (i + 1) * chunk):
            for h in range(heads):
                memory[r, h] = aux_ref[0, h, r : r + 1, :] * memory[r, h] + turned[h][:, r : r + 1] * aux_ref[2, h, r : r + 1, :]
        stores[i].start()
    for store in stores:
        store.wait()


def per_device(
    mesh, tokens, norm_gain, w_query, w_key, w_value, w_outgate, w_input_gate, w_forget_gate,
    memory, normalizer, memory_max, w_output, ffn_gain, w_gate, w_up, w_down,
):
    n, nt = mesh.shape["kv"], mesh.shape["tp"]
    nz, ny = split_groups(n)
    own, cols = tokens.shape
    heads, dim = memory.shape[1], memory.shape[2]
    inner = heads * dim
    ff = w_down.shape[0]
    pad = -(-ff // 128) * 128
    dma = pltpu.SemaphoreType.DMA
    peers = max(nt - 1, 1)
    w_gate, w_up = w_gate.T, w_up.T
    vm = lambda like: pltpu.VMEM(like.shape, like.dtype)
    result, aux, new_max = pl.pallas_call(
        functools.partial(step_kernel, nz, ny, nt, cols * nt),
        out_shape=(
            jax.ShapeDtypeStruct((own, cols), BF16),
            jax.ShapeDtypeStruct((3, heads, own, dim), F32),
            jax.ShapeDtypeStruct((own, heads), F32),
        ),
        in_specs=[VMEM] * 7 + [ANY] * 9,
        out_specs=(VMEM, VMEM, VMEM),
        scratch_shapes=[
            vm(w_key), vm(w_value), vm(w_query), vm(w_outgate),
            pltpu.VMEM((heads, own, dim, dim), F32),
            vm(w_output), vm(w_gate), vm(w_up), vm(w_down),
            pltpu.VMEM((peers, own, cols), BF16),
            pltpu.VMEM((own, cols * nt), BF16),
            pltpu.VMEM((own, dim), F32),
            pltpu.VMEM((own, inner), BF16),
            pltpu.VMEM((peers, own, inner), BF16),
            pltpu.VMEM((n, own, cols), BF16),
            pltpu.VMEM((nz, ny * own, 2 * pad + 128), BF16),
            pltpu.VMEM((nz, peers, ny * own, 2 * pad + 128), BF16),
            pltpu.VMEM((nz, ny, own, cols), BF16),
            pltpu.VMEM((nz, ny, own, cols), BF16),
            pltpu.VMEM((nz, own, cols), BF16),
            pltpu.VMEM((nz, own, cols), BF16),
            dma((8 + heads,)),
            dma((peers, 2)),
            dma((peers, 2)),
            dma((nz, 2)),
            dma((nz, ny, 2)),
            dma((nz, peers, 2)),
            dma((nz, ny, 2)),
            dma((nz, 2)),
        ],
        compiler_params=pltpu.CompilerParams(collective_id=0, has_side_effects=True),
        name="decode_step",
    )(
        tokens, norm_gain.reshape(1, -1), w_input_gate.T, w_forget_gate.T, normalizer, memory_max,
        ffn_gain.reshape(1, cols), w_key, w_value, w_query, w_outgate, memory, w_output, w_gate, w_up, w_down,
    )
    chunk = 2 if own % 2 == 0 else 1
    new_memory, new_normalizer, new_max, result = pl.pallas_call(
        functools.partial(update_kernel, chunk),
        out_shape=(
            jax.ShapeDtypeStruct(memory.shape, F32),
            jax.ShapeDtypeStruct(normalizer.shape, F32),
            jax.ShapeDtypeStruct(memory_max.shape, F32),
            jax.ShapeDtypeStruct(tokens.shape, BF16),
        ),
        in_specs=[ANY, VMEM, VMEM, VMEM, VMEM],
        out_specs=(ANY, VMEM, VMEM, VMEM),
        scratch_shapes=[vm(memory), dma((own // chunk,)), dma((own // chunk,))],
        name="memory_update",
    )(memory, aux, normalizer, new_max, result)
    return (result, new_memory, new_normalizer, new_max)


def solution(mesh):
    placed = (
        P("kv", "tp"),
        P(),
        P(None, "tp"),
        P(None, "tp"),
        P(None, "tp"),
        P(None, "tp"),
        P(),
        P(),
        P("kv", "tp", None, None),
        P("kv", "tp", None),
        P("kv", "tp"),
        P(None, "tp"),
        P("tp"),
        P("tp", "kv"),
        P("tp", "kv"),
        P("kv", "tp"),
    )
    return jax.shard_map(
        functools.partial(per_device, mesh),
        mesh=mesh,
        in_specs=placed,
        out_specs=(P("kv", "tp"), P("kv", "tp", None, None), P("kv", "tp", None), P("kv", "tp")),
        check_vma=False,
    )
```

time: 59.2 us -> 45.1 us (0.76)
  matrix products: 12.8 us -> 0 us
  Pallas kernels: 30 us -> 41.4 us
  other arithmetic: 6.76 us -> 0 us
  local copies, waits for them, and re-layouts: 5.88 us -> 2.7 us
  blocking collectives: 2.34 us -> 0 us
    dot_general x7 -> x0, matrix products: 12.8 us -> none  [the longest x4 5.58 us: project(): jnp.dot(normed, weight, preferred_element_type=jnp.float32)]
    pallas_call x1 -> x2, Pallas kernels: 30 us -> 41.4 us  [the longest x1 36.2 us: per_device(): pl.pallas_call(functools.partial(step_kernel, nz, ny, nt, cols * nt), out...]
    add x1 -> x0, other arithmetic: 4.73 us -> none  [per_device(): keep_weight[..., None, None] * memory]
    unnamed x16 -> x2, local copies, waits for them, and re-layouts: 5.46 us -> 2.7 us
    all_gather x1 -> x0, blocking collectives: 2.34 us -> none  [per_device(): full_rows = lax.all_gather(tokens, 'tp', axis=1, tiled=True)]
    reduce_sum x4 -> x0, other arithmetic: 1.18 us -> none  [the longest x1 0.72 us: per_device(): denominator = jnp.sum(queries * new_normalizer, axis=-1)]
    exp x2 -> x0, other arithmetic: 0.72 us -> none  [the longest x1 0.71 us: per_device(): keep_weight = jnp.exp(lforget + memory_max - new_max)]
where the time goes in v2:
time: 45.1 us; the launch traced here: 44.8 us
  Pallas kernels  41.4 us (92%)
  local copies, waits for them, and re-layouts  2.7 us (6%)
  between operations  0.65 us (1%)
    pallas_call x1, Pallas kernels, per_device(): pl.pallas_call(functools.partial(step_kernel, nz, ny, nt, cols * nt), out...  36.2 us
    pallas_call x1, Pallas kernels, per_device(): pl.pallas_call(functools.partial(update_kernel, chunk), out_shape=(jax.Sh...  5.2 us
    unnamed x2, local copies, waits for them, and re-layouts  2.7 us

profile of v2, /device:TPU:0, one launch (start us, length us, event | category | flops | bytes accessed | tf_op | source)
XLA Modules:
  0.0 44.8 jit_solution(3578378821465322024)
XLA Ops:
  0.6 1.4 %copy.20.memory_max_ref = f32[16,4]{1,0:T(8,128)} copy(f32[16,4]{0,1:T(4,128)} %param.26) | data formatting | bytes 512 | tf_op args[10]
  2.0 36.2 %decode_step.1 = (bf16[16,1024]{1,0:T(8,128)(2,1)}, f32[3,4,16,128]{3,2,1,0:T(8,128)}, f32[16,4]{1,0:T(8,128)}) custom-call(bf16[16,1024]{1,0:T(8,128)(2,1)} %tokens_ref.1, f32[1,2048]{1,0:T(1,128)} %bitcast.10, bf16[8,2048]{1,0:T(8,128)(2,1)} %bitcast.8, bf16[8,2048]{1,0:T(8,128)(2,1)} %bitcast.9, f32[16,4,128]{2,1,0:T(4,128)} %normalizer_ref.3, ...), custom_call_target="tpu_custom_call" | custom-call | tf_op jit(solution)/shard_map/decode_step/pallas_call | solution.py:285
  38.2 5.2 %memory_update.1 = (f32[16,4,128,128]{3,2,1,0:T(8,128)}, f32[16,4,128]{2,1,0:T(4,128)}, f32[16,4]{1,0:T(8,128)}, bf16[16,1024]{1,0:T(8,128)(2,1)}) custom-call(f32[16,4,128,128]{3,2,1,0:T(8,128)} %memory_hbm.3, f32[3,4,16,128]{3,2,1,0:T(8,128)} %get-tuple-element.11.aux_ref, f32[16,4,128]{2,1,0:T(4,128)} %normalizer_ref.3, ...), custom_call_target="tpu_custom_call" | custom-call | tf_op jit(solution)/shard_map/memory_update/pallas_call | solution.py:326
  43.4 1.3 %copy.21 = f32[16,4]{0,1:T(4,128)} copy(f32[16,4]{1,0:T(8,128)} %get-tuple-element.21) | data formatting | bytes 512

commit v3 on v2

--- a/solution.py
+++ b/solution.py
@@ -120,14 +120,16 @@
     queries = projected(2, w_query) * dim ** (-0.5)
     outgates = projected(3, w_outgate)
     lane = lax.broadcasted_iota(jnp.int32, igates.shape, 1)
+    diagonal = lax.broadcasted_iota(jnp.int32, (own, own), 0) == lax.broadcasted_iota(jnp.int32, (own, own), 1)
     for h in range(heads):
         mine = lane == t * heads + h
         igate = jnp.sum(jnp.where(mine, igates, 0.0), axis=-1, keepdims=True)
         forget = jnp.sum(jnp.where(mine, fgates, 0.0), axis=-1, keepdims=True)
-        carried = jnp.minimum(forget, 0.0) - jnp.log1p(jnp.exp(-jnp.abs(forget))) + memory_max_ref[:, h : h + 1]
+        carried = jnp.minimum(forget, 0.0) - jnp.log1p(jnp.exp(-jnp.abs(forget)))
+        carried = carried + jnp.sum(jnp.where(diagonal, memory_max_ref[h : h + 1, :], 0.0), axis=-1, keepdims=True)
         new_max = jnp.maximum(carried, igate)
         keep_weight = jnp.exp(carried - new_max)
-        new_max_ref[:, h : h + 1] = new_max
+        new_max_ref[h : h + 1, :] = jnp.sum(jnp.where(diagonal, new_max, 0.0), axis=0, keepdims=True)
         at = slice(h * dim, (h + 1) * dim)
         key, value, query = jnp.exp(igate - new_max) * keys[:, at], values[:, at], queries[:, at]
         keep_wide = jnp.broadcast_to(keep_weight, key.shape)
@@ -203,7 +205,7 @@
         scale = lax.rsqrt(square / width + 1e-06)
         g = scale * gate
         hidden = (g / (1.0 + jnp.exp(-g)) * (scale * up)).astype(BF16)
-        if off == 0:
+        if off == min(1, nz - 1):
             arrived(first + 3)
         out = jnp.dot(hidden, w_down[...], preferred_element_type=F32)
         down[off] = out.reshape(ny, own, cols).astype(BF16)
@@ -227,13 +229,17 @@
     stage_a(0)
     for o in range(2, nz):
         spread(o)
-    for o in range(0, nz + 2):
-        if 1 <= o + 1 < nz:
-            stage_a(o + 1)
+    for o in range(1, nz + 1):
         if o < nz:
-            stage_b(o)
-        if 0 <= o - 1 < nz:
-            stage_c(o - 1)
+            stage_a(o)
+        if o > 1:
+            stage_b(o - 1)
+        if o > 2:
+            stage_c(o - 2)
+    stage_b(0)
+    if nz > 1:
+        stage_c(nz - 1)
+    stage_c(0)
     acc = rows[k].astype(F32) + keep[0]
     for o in range(1, nz):
         totals[o].wait_recv()
@@ -287,7 +293,7 @@
         out_shape=(
             jax.ShapeDtypeStruct((own, cols), BF16),
             jax.ShapeDtypeStruct((3, heads, own, dim), F32),
-            jax.ShapeDtypeStruct((own, heads), F32),
+            jax.ShapeDtypeStruct((heads, own), F32),
         ),
         in_specs=[VMEM] * 7 + [ANY] * 9,
         out_specs=(VMEM, VMEM, VMEM),
@@ -319,7 +325,7 @@
         compiler_params=pltpu.CompilerParams(collective_id=0, has_side_effects=True),
         name="decode_step",
     )(
-        tokens, norm_gain.reshape(1, -1), w_input_gate.T, w_forget_gate.T, normalizer, memory_max,
+        tokens, norm_gain.reshape(1, -1), w_input_gate.T, w_forget_gate.T, normalizer, memory_max.T,
         ffn_gain.reshape(1, cols), w_key, w_value, w_query, w_outgate, memory, w_output, w_gate, w_up, w_down,
     )
     chunk = 2 if own % 2 == 0 else 1
@@ -328,7 +334,7 @@
         out_shape=(
             jax.ShapeDtypeStruct(memory.shape, F32),
             jax.ShapeDtypeStruct(normalizer.shape, F32),
-            jax.ShapeDtypeStruct(memory_max.shape, F32),
+            jax.ShapeDtypeStruct((heads, own), F32),
             jax.ShapeDtypeStruct(tokens.shape, BF16),
         ),
         in_specs=[ANY, VMEM, VMEM, VMEM, VMEM],
@@ -336,7 +342,7 @@
         scratch_shapes=[vm(memory), dma((own // chunk,)), dma((own // chunk,))],
         name="memory_update",
     )(memory, aux, normalizer, new_max, result)
-    return (result, new_memory, new_normalizer, new_max)
+    return (result, new_memory, new_normalizer, new_max.T)
 
 
 def solution(mesh):

time: 45.1 us -> 42 us (0.931)
  local copies, waits for them, and re-layouts: 2.7 us -> 0 us
    unnamed x2 -> x0, local copies, waits for them, and re-layouts: 2.7 us -> none
where the time goes in v3:
time: 42 us; the launch traced here: 41.8 us
  Pallas kernels  41.2 us (98%)
  between operations  0.64 us (2%)
    pallas_call x1, Pallas kernels, per_device(): pl.pallas_call(functools.partial(step_kernel, nz, ny, nt, cols * nt), out...  36 us
    pallas_call x1, Pallas kernels, per_device(): pl.pallas_call(functools.partial(update_kernel, chunk), out_shape=(jax.Sh...  5.2 us

profile of v3, /device:TPU:0, one launch (start us, length us, event | category | flops | bytes accessed | tf_op | source)
XLA Modules:
  0.0 41.8 jit_solution(13388604215299061388)
XLA Ops:
  0.6 36.0 %decode_step.1 = (bf16[16,1024]{1,0:T(8,128)(2,1)}, f32[3,4,16,128]{3,2,1,0:T(8,128)}, f32[4,16]{1,0:T(4,128)}) custom-call(bf16[16,1024]{1,0:T(8,128)(2,1)} %tokens_ref.1, f32[1,2048]{1,0:T(1,128)} %bitcast.12, bf16[8,2048]{1,0:T(8,128)(2,1)} %bitcast.10, bf16[8,2048]{1,0:T(8,128)(2,1)} %bitcast.11, f32[16,4,128]{2,1,0:T(4,128)} %normalizer_ref.3, ...), custom_call_target="tpu_custom_call" | custom-call | tf_op jit(solution)/shard_map/decode_step/pallas_call | solution.py:291
  36.6 5.2 %memory_update.1 = (f32[16,4,128,128]{3,2,1,0:T(8,128)}, f32[16,4,128]{2,1,0:T(4,128)}, f32[4,16]{1,0:T(4,128)}, bf16[16,1024]{1,0:T(8,128)(2,1)}) custom-call(f32[16,4,128,128]{3,2,1,0:T(8,128)} %memory_hbm.3, f32[3,4,16,128]{3,2,1,0:T(8,128)} %get-tuple-element.11.aux_ref, f32[16,4,128]{2,1,0:T(4,128)} %normalizer_ref.3, ...), custom_call_target="tpu_custom_call" | custom-call | tf_op jit(solution)/shard_map/memory_update/pallas_call | solution.py:332
